TPU v7x, 32 devices: a whole 2x2x4 slice. The times are simulated.
32 devices in a mesh: rep: 4 (over z), fs: 2 (over y), tp: 4 (over x, core).
Axes of the slice: x: 2, y: 2, z: 4, core: 2. Of those that a mesh axis runs over, the one named last changes fastest.
Arguments:
- layer_input: bfloat16 [3072, 2048], P('rep', ('fs', 'tp')), may hold values from -0.8046875 to 0.8046875
- gate_saved: bfloat16 [3072, 5120], P('rep', 'tp'), may hold values from -6 to 6
- up_saved: bfloat16 [3072, 5120], P('rep', 'tp'), may hold values from -6 to 6
- out_grad: bfloat16 [3072, 2048], P('rep'), may hold values from -0.8046875 to 0.8046875
- conv_taps: bfloat16 [3, 5120], P(None, 'tp'), may hold values from -3.5 to 3.5
- w_gate: bfloat16 [2048, 5120], P('fs', 'tp'), may hold values from -0.125 to 0.125
- w_up: bfloat16 [2048, 5120], P('fs', 'tp'), may hold values from -0.125 to 0.125
- w_down: bfloat16 [5120, 2048], P('tp', 'fs'), may hold values from -0.078125 to 0.078125
Outputs:
- input_grad: bfloat16 [3072, 2048], P('rep', ('fs', 'tp'))
- gate_grad: float32 [2048, 5120], P('fs', 'tp')
- up_grad: float32 [2048, 5120], P('fs', 'tp')
- down_grad: float32 [5120, 2048], P('tp', 'fs')
- taps_grad: float32 [3, 5120], P(None, 'tp')
All inputs are finite; a program needn't handle non-finite values.
Results may differ from a plain program's by a relative error of at most 0.018.
Values may be sent and summed in bfloat16 or wider, within the bound.
A program may use at most 128 MiB of HBM per device.

v0:
```python
import functools

import jax
import jax.numpy as jnp
from jax import lax
from jax.experimental import pallas as pl
from jax.experimental.pallas import tpu as pltpu
from jax.sharding import PartitionSpec as P

MESH = pl.DeviceIdType.MESH
F32 = jnp.float32
BF16 = jnp.bfloat16
CH = 128
HALF = CH // 2


def kernel(n_rep, n_fs, n_tp, x_in, gate_in, up_in, og_in, taps_in, wg_in, wu_in, wd_in,
           grads_out, ig_out, taps_out,
           xb, gate, up, og, wg, wu, wd, part, from_out, from_in, gp, upp, terms, terms_in, taps_all,
           xs_sem, xr_sem, gl_sem, ul_sem, ld_sem, wl_sem, ws_sem, wr_sem,
           in_s, in_r, out_s, out_r, st_sem, ts_sem, tr_sem, ps_sem, pr_sem):
    rep, fs, tp = lax.axis_index("rep"), lax.axis_index("fs"), lax.axis_index("tp")
    seq, hid = gate.shape
    dw = wd_in.shape[1]
    w = x_in.shape[1]
    nj = hid // CH
    half = n_rep // 2
    low = rep < half
    depth = jnp.where(low, rep, n_rep - 1 - rep)
    inward = jnp.where(low, rep + 1, rep - 1)
    outward = jnp.where(low, rep - 1, rep + 1)
    has_out = depth > 0
    outward = jnp.where(has_out, outward, inward)
    innermost = depth == half - 1
    lag = 1 + 18 * (half - 1 - depth)
    lead = min(4, nj)
    steps = 3 * nj

    def rows(j):
        return pl.ds(pl.multiple_of(j * CH, CH), CH)

    def piece(i):
        return pl.ds(pl.multiple_of(i * HALF, HALF), HALF)

    def unit(i):
        v, h = lax.div(i, 2), lax.rem(i, 2)
        a = v - lead
        b = a - 3 * (nj - lead)
        m = lax.rem(a, 3)
        mid = a < 3 * (nj - lead)
        first = a < 0
        k = jnp.where(first, 0, jnp.where(mid, jnp.where(m == 2, 0, m + 1), 1 + lax.rem(b, 2)))
        j = jnp.where(first, v, jnp.where(
            mid, lax.div(a, 3) + jnp.where(m == 2, lead, 0), nj - lead + lax.div(b, 2)))
        return 2 * j + h, k

    def fs_peer(d):
        return lax.rem(fs + d, n_fs)

    def tp_peer(d):
        return lax.rem(tp + d, n_tp)

    def load_gate(j):
        return pltpu.make_async_copy(gate_in.at[:, rows(j)], gate.at[:, rows(j)], gl_sem.at[j])

    def load_up(j):
        return pltpu.make_async_copy(up_in.at[:, rows(j)], up.at[:, rows(j)], ul_sem.at[j])

    def load_wd(j):
        return pltpu.make_async_copy(wd_in.at[rows(j), :], wd.at[fs, rows(j), :], wl_sem.at[j])

    def send_wd(j, d):
        return pltpu.make_async_remote_copy(
            src_ref=wd_in.at[rows(j), :], dst_ref=wd.at[fs, rows(j), :],
            send_sem=ws_sem.at[d - 1, j], recv_sem=wr_sem.at[d - 1, j],
            device_id={"fs": fs_peer(d)}, device_id_type=MESH)

    def recv_wd(j, d):
        src = lax.rem(fs + n_fs - d, n_fs)
        return pltpu.make_async_remote_copy(
            src_ref=wd_in.at[rows(j), :], dst_ref=wd.at[src, rows(j), :],
            send_sem=ws_sem.at[d - 1, j], recv_sem=wr_sem.at[d - 1, j],
            device_id={"fs": fs_peer(d)}, device_id_type=MESH)

    def x_copy(d, slot):
        return pltpu.make_async_remote_copy(
            src_ref=x_in, dst_ref=xb.at[slot], send_sem=xs_sem.at[d - 1], recv_sem=xr_sem.at[d - 1],
            device_id={"tp": tp_peer(d)}, device_id_type=MESH)

    def term_copy(d):
        return pltpu.make_async_remote_copy(
            src_ref=terms.at[tp_peer(d)], dst_ref=terms_in.at[d - 1],
            send_sem=ts_sem.at[d - 1], recv_sem=tr_sem.at[d - 1],
            device_id={"tp": tp_peer(d)}, device_id_type=MESH)

    def taps_copy(d, slot):
        return pltpu.make_async_remote_copy(
            src_ref=taps_all.at[rep], dst_ref=taps_all.at[slot],
            send_sem=ps_sem.at[d - 1], recv_sem=pr_sem.at[d - 1],
            device_id={"rep": lax.rem(rep + d, n_rep)}, device_id_type=MESH)

    def in_copy(j, k, dst):
        return pltpu.make_async_remote_copy(
            src_ref=part.at[k, piece(j), :], dst_ref=dst.at[k, piece(j), :],
            send_sem=in_s.at[k, j], recv_sem=(in_r if dst is from_out else out_r).at[k, j],
            device_id={"rep": inward}, device_id_type=MESH)

    def out_copy(j, k):
        return pltpu.make_async_remote_copy(
            src_ref=from_in.at[k, piece(j), :], dst_ref=from_in.at[k, piece(j), :],
            send_sem=out_s.at[k, j], recv_sem=out_r.at[k, j],
            device_id={"rep": outward}, device_id_type=MESH)

    def store(j, k):
        return pltpu.make_async_copy(from_in.at[k, piece(j), :], grads_out.at[k, piece(j), :], st_sem.at[k, j])

    loads = [
        pltpu.make_async_copy(og_in, og, ld_sem.at[0]),
        pltpu.make_async_copy(wg_in, wg, ld_sem.at[1]),
        pltpu.make_async_copy(wu_in, wu, ld_sem.at[2]),
        pltpu.make_async_copy(x_in, xb.at[tp], ld_sem.at[3]),
    ]
    load_gate(0).start()
    load_up(0).start()
    loads[0].start()
    load_wd(0).start()
    loads[3].start()

    barrier = pltpu.get_barrier_semaphore()
    for axis, n, me in (("rep", n_rep, rep), ("fs", n_fs, fs), ("tp", n_tp, tp)):
        for d in range(1, n):
            pl.semaphore_signal(barrier, inc=1, device_id={axis: lax.rem(me + d, n)}, device_id_type=MESH)
    pl.semaphore_wait(barrier, n_rep + n_fs + n_tp - 3)

    for d in range(1, n_tp):
        x_copy(d, tp).start()

    def send_all(j, c):
        for d in range(1, n_fs):
            send_wd(j, d).start()
        return c
    lax.fori_loop(0, nj, send_all, 0)

    def load_rest(j, c):
        load_gate(j).start()
        load_up(j).start()
        load_wd(j).start()
        return c
    lax.fori_loop(1, nj, load_rest, 0)
    loads[1].start()
    loads[2].start()

    pos = lax.broadcasted_iota(jnp.int32, (seq, CH), 0)

    def back(v, n):
        return jnp.where(pos >= n, pltpu.roll(v, n, 0), 0.0)

    def ahead(v, n):
        return jnp.where(pos < seq - n, pltpu.roll(v, seq - n, 0), 0.0)

    def conv(j):
        g = gate[:, rows(j)].astype(F32)
        t = taps_in[:, rows(j)].astype(F32)
        b1, b2 = back(g, 1), back(g, 2)
        return g, b1, b2, t, t[0:1] * b2 + t[1:2] * b1 + t[2:3] * g

    tdot = functools.partial(lax.dot_general, dimension_numbers=(((0,), (0,)), ((), ())),
                             preferred_element_type=F32)
    wdot = functools.partial(lax.dot_general, dimension_numbers=(((1,), (1,)), ((), ())),
                             preferred_element_type=F32)

    def compute_down(j):
        load_gate(j).wait()
        load_up(j).wait()
        g, b1, b2, t, co = conv(j)
        act = (co * jax.nn.sigmoid(co) * up[:, rows(j)].astype(F32)).astype(BF16)
        cols = pl.ds(pl.multiple_of(fs * dw, dw), dw)
        part[0, rows(j), :] = tdot(act, og[:, cols]).astype(BF16)

    def compute_rest(j):
        load_wd(j).wait()
        for d in range(1, n_fs):
            recv_wd(j, d).wait_recv()
        ag = wdot(og[:, 0:dw], wd[0, rows(j), :])
        for f in range(1, n_fs):
            ag = ag + wdot(og[:, f * dw:(f + 1) * dw], wd[f, rows(j), :])
        g, b1, b2, t, co = conv(j)
        s = jax.nn.sigmoid(co)
        u_part = (ag * (co * s)).astype(BF16)
        cg = ag * up[:, rows(j)].astype(F32) * s * (1.0 + co * (1.0 - s))
        g_part = (t[0:1] * ahead(cg, 2) + t[1:2] * ahead(cg, 1) + t[2:3] * cg).astype(BF16)
        taps_all[rep, 0:1, rows(j)] = jnp.sum(cg * b2, axis=0, keepdims=True)
        taps_all[rep, 1:2, rows(j)] = jnp.sum(cg * b1, axis=0, keepdims=True)
        taps_all[rep, 2:3, rows(j)] = jnp.sum(cg * g, axis=0, keepdims=True)
        gp[:, rows(j)] = g_part
        upp[:, rows(j)] = u_part

        @pl.when(j == 0)
        def _():
            loads[3].wait()
            for d in range(1, n_tp):
                x_copy(d, lax.rem(tp + n_tp - d, n_tp)).wait_recv()
        for b in range(n_tp):
            part[1, rows(j), b * w:(b + 1) * w] = tdot(g_part, xb[b]).astype(BF16)
            part[2, rows(j), b * w:(b + 1) * w] = tdot(u_part, xb[b]).astype(BF16)

    def compute_term(d):
        @pl.when(d == 1)
        def _():
            for p in range(1, n_rep):
                taps_copy(p, rep).start()
            loads[1].wait()
            loads[2].wait()
        b = tp_peer(d)
        r = pl.ds(pl.multiple_of(b * w, w), w)
        terms[b] = (wdot(gp[...], wg[r, :]) + wdot(upp[...], wu[r, :])).astype(BF16)

        @pl.when(d < n_tp)
        def _():
            term_copy(d).start()

    def q_stage(j, k):
        @pl.when(has_out)
        def _():
            in_copy(j, k, from_out).wait_recv()
            r = piece(j)
            part[k, r, :] = (part[k, r, :].astype(F32) + from_out[k, r, :].astype(F32)).astype(BF16)

        @pl.when(innermost)
        def _():
            in_copy(j, k, from_in).start()

        @pl.when(jnp.logical_not(innermost))
        def _():
            in_copy(j, k, from_out).start()

    def s_stage(j, k):
        out_copy(j, k).wait_recv()

        @pl.when(innermost)
        def _():
            r = piece(j)
            from_in[k, r, :] = (part[k, r, :].astype(F32) + from_in[k, r, :].astype(F32)).astype(BF16)

        @pl.when(has_out)
        def _():
            out_copy(j, k).start()
        store(j, k).start()

    loads[0].wait()
    compute_down(0)

    def step(v, c):
        for h in range(2):
            i = 2 * v + h

            @pl.when(v < steps)
            def _():
                q_stage(*unit(i))
            si = i - lag

            @pl.when(jnp.logical_and(si >= 0, si < 2 * steps))
            def _():
                s_stage(*unit(si))
        a = v - (lead - 1)
        b = a - 2 * (nj - lead)
        early = a < 0
        mid = jnp.logical_and(a >= 0, b < 0)
        is_down = jnp.logical_or(early, jnp.logical_and(mid, lax.rem(a, 2) == 1))
        is_rest = jnp.logical_and(jnp.logical_not(is_down), b < lead)

        @pl.when(is_down)
        def _():
            compute_down(jnp.where(early, v + 1, lead + lax.div(a, 2)))

        @pl.when(is_rest)
        def _():
            compute_rest(jnp.where(mid, lax.div(a, 2), nj - lead + b))

        @pl.when(jnp.logical_and(b >= lead, b < lead + n_tp))
        def _():
            compute_term(b - lead + 1)
        return c
    lax.fori_loop(0, steps + 1 + 9 * (half - 1), step, 0)

    total = terms[tp].astype(F32)
    for d in range(1, n_tp):
        term_copy(d).wait_recv()
        total = total + terms_in[d - 1].astype(F32)
    ig_out[...] = total.astype(BF16)
    for d in range(1, n_rep):
        taps_copy(d, lax.rem(rep + n_rep - d, n_rep)).wait_recv()
    acc = taps_all[0]
    for i in range(1, n_rep):
        acc = acc + taps_all[i]
    taps_out[...] = acc

    for d in range(1, n_tp):
        x_copy(d, tp).wait_send()
        term_copy(d).wait_send()
    for d in range(1, n_rep):
        taps_copy(d, rep).wait_send()

    def drain(j, c):
        for d in range(1, n_fs):
            send_wd(j, d).wait_send()
        for k in range(3):
            for i in (2 * j, 2 * j + 1):
                in_copy(i, k, from_out).wait_send()
                store(i, k).wait()

                @pl.when(has_out)
                def _():
                    out_copy(i, k).wait_send()
        return c
    lax.fori_loop(0, nj, drain, 0)


def widen(grads, input_grad, taps, ig_out, gate_out, up_out, down_out, taps_out):
    down_out[...] = grads[0].astype(F32)
    gate_out[...] = grads[1].astype(F32).T
    up_out[...] = grads[2].astype(F32).T

    @pl.when(pl.program_id(0) == 0)
    def _():
        ig_out[...] = input_grad[...]
        taps_out[...] = taps[0:3, :]


def solution(mesh):
    n_rep, n_fs, n_tp = mesh.shape["rep"], mesh.shape["fs"], mesh.shape["tp"]

    def local(layer_input, gate_saved, up_saved, out_grad, conv_taps, w_gate, w_up, w_down):
        seq, w = layer_input.shape
        dw, hid = w_gate.shape
        width = out_grad.shape[1]
        nj = hid // CH
        any_spec = pl.BlockSpec(memory_space=pl.ANY)
        vmem = pl.BlockSpec(memory_space=pltpu.VMEM)
        dma = pltpu.SemaphoreType.DMA
        grads, input_grad, taps = pl.pallas_call(
            functools.partial(kernel, n_rep, n_fs, n_tp),
            out_shape=(
                jax.ShapeDtypeStruct((3, hid, dw), BF16),
                jax.ShapeDtypeStruct((seq, w), BF16),
                jax.ShapeDtypeStruct((8, hid), F32),
            ),
            in_specs=[any_spec] * 4 + [vmem] + [any_spec] * 3,
            out_specs=(any_spec, vmem, vmem),
            scratch_shapes=[
                pltpu.VMEM((n_tp, seq, w), BF16),
                pltpu.VMEM((seq, hid), BF16),
                pltpu.VMEM((seq, hid), BF16),
                pltpu.VMEM((seq, width), BF16),
                pltpu.VMEM((dw, hid), BF16),
                pltpu.VMEM((dw, hid), BF16),
                pltpu.VMEM((n_fs, hid, dw), BF16),
                pltpu.VMEM((3, hid, dw), BF16),
                pltpu.VMEM((3, hid, dw), BF16),
                pltpu.VMEM((3, hid, dw), BF16),
                pltpu.VMEM((seq, hid), BF16),
                pltpu.VMEM((seq, hid), BF16),
                pltpu.VMEM((n_tp, seq, w), BF16),
                pltpu.VMEM((n_tp - 1, seq, w), BF16),
                pltpu.VMEM((n_rep, 8, hid), F32),
                dma((n_tp - 1,)),
                dma((n_tp - 1,)),
                dma((nj,)),
                dma((nj,)),
                dma((4,)),
                dma((nj,)),
                dma((n_fs - 1, nj)),
                dma((n_fs - 1, nj)),
                dma((3, 2 * nj)),
                dma((3, 2 * nj)),
                dma((3, 2 * nj)),
                dma((3, 2 * nj)),
                dma((3, 2 * nj)),
                dma((n_tp - 1,)),
                dma((n_tp - 1,)),
                dma((n_rep - 1,)),
                dma((n_rep - 1,)),
            ],
            compiler_params=pltpu.CompilerParams(
                collective_id=0, has_side_effects=True, vmem_limit_bytes=67043328
            ),
        )(layer_input, gate_saved, up_saved, out_grad, conv_taps, w_gate, w_up, w_down)
        step = 2 * CH if hid % (2 * CH) == 0 else CH

        def whole(shape):
            return pl.BlockSpec(shape, lambda i: (0, 0))
        wide = pl.BlockSpec((dw, step), lambda i: (0, i))
        return pl.pallas_call(
            widen,
            grid=(hid // step,),
            out_shape=(
                jax.ShapeDtypeStruct((seq, w), BF16),
                jax.ShapeDtypeStruct((dw, hid), F32),
                jax.ShapeDtypeStruct((dw, hid), F32),
                jax.ShapeDtypeStruct((hid, dw), F32),
                jax.ShapeDtypeStruct((3, hid), F32),
            ),
            in_specs=[
                pl.BlockSpec((3, step, dw), lambda i: (0, i, 0)), whole((seq, w)), whole((8, hid)),
            ],
            out_specs=(
                whole((seq, w)), wide, wide, pl.BlockSpec((step, dw), lambda i: (i, 0)), whole((3, hid)),
            ),
        )(grads, input_grad, taps)

    return jax.shard_map(
        local,
        mesh=mesh,
        in_specs=(
            P("rep", ("fs", "tp")), P("rep", "tp"), P("rep", "tp"), P("rep", None),
            P(None, "tp"), P("fs", "tp"), P("fs", "tp"), P("tp", "fs"),
        ),
        out_specs=(P("rep", ("fs", "tp")), P("fs", "tp"), P("fs", "tp"), P("tp", "fs"), P(None, "tp")),
        check_vma=False,
    )
```

profile of v0, /device:TPU:0, one launch (start us, length us, event | category | flops | bytes accessed | tf_op | source)
XLA Modules:
  0.0 218.0 jit_solution(1028394626540451672)
XLA Ops:
  0.6 207.4 %shard_map.119 = (bf16[3,1280,1024]{2,1,0:T(8,128)(2,1)}, bf16[768,256]{1,0:T(8,128)(2,1)}, f32[8,1280]{1,0:T(8,128)}) custom-call(bf16[768,256]{1,0:T(8,128)(2,1)} %x_in.1, bf16[768,1280]{1,0:T(8,128)(2,1)} %gate_in.1, bf16[768,1280]{1,0:T(8,128)(2,1)} %up_in.1, bf16[768,2048]{1,0:T(8,128)(2,1)} %og_in.1, bf16[3,1280]{1,0:T(4,128)(2,1)} %taps_in.1, ...), custom_call_target="tpu_custom_call" | custom-call | tf_op jit(solution)/shard_map/pallas_call | solution.py:341
  208.1 10.0 %shard_map.120 = (bf16[768,256]{1,0:T(8,128)(2,1)}, f32[1024,1280]{1,0:T(8,128)}, f32[1024,1280]{1,0:T(8,128)}, f32[1280,1024]{1,0:T(8,128)}, f32[3,1280]{1,0:T(4,128)}) custom-call(bf16[3,1280,1024]{2,1,0:T(8,128)(2,1)} %get-tuple-element.8.grads, bf16[768,256]{1,0:T(8,128)(2,1)} %get-tuple-element.9.input_grad, f32[8,1280]{1,0:T(8,128)} %get-tuple-element.10.taps), custom_call_target="tpu_custom_call" | custom-call | tf_op jit(solution)/shard_map/pallas_call | solution.py:393
where the time goes:
time: 218 us
  Pallas kernels  217 us (100%)
    pallas_call x1, Pallas kernels, local(): pl.pallas_call(functools.partial(kernel, n_rep, n_fs, n_tp), out_shape=(j...  207 us
    pallas_call x1, Pallas kernels, local(): pl.pallas_call(widen, grid=(hid // step,), out_shape=(jax.ShapeDtypeStruc...  9.97 us

commit v1 on v0

--- a/solution.py
+++ b/solution.py
@@ -15,10 +15,10 @@
 
 
 def kernel(n_rep, n_fs, n_tp, x_in, gate_in, up_in, og_in, taps_in, wg_in, wu_in, wd_in,
-           grads_out, ig_out, taps_out,
-           xb, gate, up, og, wg, wu, wd, part, from_out, from_in, gp, upp, terms, terms_in, taps_all,
+           from_in, ig_out, taps_out,
+           xb, gate, up, og, wg, wu, wd, part, from_out, gp, upp, terms, terms_in, taps_all,
            xs_sem, xr_sem, gl_sem, ul_sem, ld_sem, wl_sem, ws_sem, wr_sem,
-           in_s, in_r, out_s, out_r, st_sem, ts_sem, tr_sem, ps_sem, pr_sem):
+           in_s, in_r, out_s, out_r, ts_sem, tr_sem, ps_sem, pr_sem):
     rep, fs, tp = lax.axis_index("rep"), lax.axis_index("fs"), lax.axis_index("tp")
     seq, hid = gate.shape
     dw = wd_in.shape[1]
@@ -32,7 +32,7 @@
     has_out = depth > 0
     outward = jnp.where(has_out, outward, inward)
     innermost = depth == half - 1
-    lag = 1 + 18 * (half - 1 - depth)
+    lag = 2 + 18 * (half - 1 - depth)
     lead = min(4, nj)
     steps = 3 * nj
 
@@ -110,9 +110,6 @@
             src_ref=from_in.at[k, piece(j), :], dst_ref=from_in.at[k, piece(j), :],
             send_sem=out_s.at[k, j], recv_sem=out_r.at[k, j],
             device_id={"rep": outward}, device_id_type=MESH)
-
-    def store(j, k):
-        return pltpu.make_async_copy(from_in.at[k, piece(j), :], grads_out.at[k, piece(j), :], st_sem.at[k, j])
 
     loads = [
         pltpu.make_async_copy(og_in, og, ld_sem.at[0]),
@@ -245,7 +242,6 @@
         @pl.when(has_out)
         def _():
             out_copy(j, k).start()
-        store(j, k).start()
 
     loads[0].wait()
     compute_down(0)
@@ -281,7 +277,7 @@
         def _():
             compute_term(b - lead + 1)
         return c
-    lax.fori_loop(0, steps + 1 + 9 * (half - 1), step, 0)
+    lax.fori_loop(0, steps + (2 + 1) // 2 + 9 * (half - 1), step, 0)
 
     total = terms[tp].astype(F32)
     for d in range(1, n_tp):
@@ -307,7 +303,6 @@
         for k in range(3):
             for i in (2 * j, 2 * j + 1):
                 in_copy(i, k, from_out).wait_send()
-                store(i, k).wait()
 
                 @pl.when(has_out)
                 def _():
@@ -341,12 +336,12 @@
         grads, input_grad, taps = pl.pallas_call(
             functools.partial(kernel, n_rep, n_fs, n_tp),
             out_shape=(
-                jax.ShapeDtypeStruct((3, hid, dw), BF16),
-                jax.ShapeDtypeStruct((seq, w), BF16),
-                jax.ShapeDtypeStruct((8, hid), F32),
+                pltpu.VMEM((3, hid, dw), BF16),
+                pltpu.VMEM((seq, w), BF16),
+                pltpu.VMEM((8, hid), F32),
             ),
             in_specs=[any_spec] * 4 + [vmem] + [any_spec] * 3,
-            out_specs=(any_spec, vmem, vmem),
+            out_specs=(vmem, vmem, vmem),
             scratch_shapes=[
                 pltpu.VMEM((n_tp, seq, w), BF16),
                 pltpu.VMEM((seq, hid), BF16),
@@ -355,7 +350,6 @@
                 pltpu.VMEM((dw, hid), BF16),
                 pltpu.VMEM((dw, hid), BF16),
                 pltpu.VMEM((n_fs, hid, dw), BF16),
-                pltpu.VMEM((3, hid, dw), BF16),
                 pltpu.VMEM((3, hid, dw), BF16),
                 pltpu.VMEM((3, hid, dw), BF16),
                 pltpu.VMEM((seq, hid), BF16),
@@ -375,16 +369,16 @@
                 dma((3, 2 * nj)),
                 dma((3, 2 * nj)),
                 dma((3, 2 * nj)),
-                dma((3, 2 * nj)),
                 dma((n_tp - 1,)),
                 dma((n_tp - 1,)),
                 dma((n_rep - 1,)),
                 dma((n_rep - 1,)),
             ],
             compiler_params=pltpu.CompilerParams(
-                collective_id=0, has_side_effects=True, vmem_limit_bytes=67043328
+                collective_id=0, has_side_effects=True, vmem_limit_bytes=52 * 2**20
             ),
         )(layer_input, gate_saved, up_saved, out_grad, conv_taps, w_gate, w_up, w_down)
+        grads, input_grad, taps = (pltpu.with_memory_space_constraint(v, pltpu.VMEM) for v in (grads, input_grad, taps))
         step = 2 * CH if hid % (2 * CH) == 0 else CH
 
         def whole(shape):
@@ -406,6 +400,7 @@
             out_specs=(
                 whole((seq, w)), wide, wide, pl.BlockSpec((step, dw), lambda i: (i, 0)), whole((3, hid)),
             ),
+            compiler_params=pltpu.CompilerParams(vmem_limit_bytes=24 * 2**20),
         )(grads, input_grad, taps)
 
     return jax.shard_map(

time: 218 us -> 201 us (0.922)
  Pallas kernels: 217 us -> 200 us
    pallas_call x1, Pallas kernels: 207 us -> 193 us  [local(): pl.pallas_call(functools.partial(kernel, n_rep, n_fs, n_tp), out_shape=(p...]
    pallas_call x1, Pallas kernels: 9.97 us -> 6.48 us  [local(): pl.pallas_call(widen, grid=(hid // step,), out_shape=(jax.ShapeDtypeStruc...]
where the time goes in v1:
time: 201 us; the launch traced here: 200 us
  Pallas kernels  200 us (100%)
    pallas_call x1, Pallas kernels, local(): pl.pallas_call(functools.partial(kernel, n_rep, n_fs, n_tp), out_shape=(p...  193 us
    pallas_call x1, Pallas kernels, local(): pl.pallas_call(widen, grid=(hid // step,), out_shape=(jax.ShapeDtypeStruc...  6.48 us

profile of v1, /device:TPU:0, one launch (start us, length us, event | category | flops | bytes accessed | tf_op | source)
XLA Modules:
  0.0 200.3 jit_solution(2613893931580867464)
XLA Ops:
  0.6 193.2 %shard_map.119 = (bf16[3,1280,1024]{2,1,0:T(8,128)(2,1)S(1)}, bf16[768,256]{1,0:T(8,128)(2,1)S(1)}, f32[8,1280]{1,0:T(8,128)S(1)}) custom-call(bf16[768,256]{1,0:T(8,128)(2,1)} %x_in.1, bf16[768,1280]{1,0:T(8,128)(2,1)} %gate_in.1, bf16[768,1280]{1,0:T(8,128)(2,1)} %up_in.1, bf16[768,2048]{1,0:T(8,128)(2,1)} %og_in.1, bf16[3,1280]{1,0:T(4,128)(2,1)} %taps_in.1, ...), custom_call_target="tpu_custom_call" | custom-call | tf_op jit(solution)/shard_map/pallas_call | solution.py:336
  193.8 6.5 %shard_map.120 = (bf16[768,256]{1,0:T(8,128)(2,1)}, f32[1024,1280]{1,0:T(8,128)}, f32[1024,1280]{1,0:T(8,128)}, f32[1280,1024]{1,0:T(8,128)}, f32[3,1280]{1,0:T(4,128)}) custom-call(bf16[3,1280,1024]{2,1,0:T(8,128)(2,1)S(1)} %get-tuple-element.8.grads, bf16[768,256]{1,0:T(8,128)(2,1)S(1)} %get-tuple-element.9.input_grad, f32[8,1280]{1,0:T(8,128)S(1)} %get-tuple-element.10.taps), custom_call_target="tpu_custom_call" | custom-call | tf_op jit(solution)/shard_map/pallas_call | solution.py:387

commit v2 on v1

v2 whole, which is shorter than its diff:
```python
import functools

import jax
import jax.numpy as jnp
from jax import lax
from jax.experimental import pallas as pl
from jax.experimental.pallas import tpu as pltpu
from jax.sharding import PartitionSpec as P

MESH = pl.DeviceIdType.MESH
F32 = jnp.float32
BF16 = jnp.bfloat16
CH = 128
SUB = 4
HALF = CH // SUB
LAG = 3
WIDE = 128


def kernel(n_rep, n_fs, n_tp, x_in, gate_in, up_in, og_in, taps_in, wg_in, wu_in, wd_in,
           from_in, ig_out, taps_out,
           xb, gate, up, og, wt, wg, wu, wd, act, part, from_out, gp, upp, terms, terms_in, taps_own, taps_all,
           xs_sem, xr_sem, gl_sem, ul_sem, ld_sem, wl_sem, ws_sem, wr_sem,
           in_s, in_r, out_s, out_r, ts_sem, tr_sem, ps_sem, pr_sem):
    rep, fs, tp = lax.axis_index("rep"), lax.axis_index("fs"), lax.axis_index("tp")
    seq, hid = gate.shape
    dw = wd_in.shape[1]
    w = x_in.shape[1]
    nj = hid // CH
    half = n_rep // 2
    low = rep < half
    depth = jnp.where(low, rep, n_rep - 1 - rep)
    inward = jnp.where(low, rep + 1, rep - 1)
    outward = jnp.where(low, rep - 1, rep + 1)
    has_out = depth > 0
    outward = jnp.where(has_out, outward, inward)
    innermost = depth == half - 1
    lag = LAG + 9 * SUB * (half - 1 - depth)
    lead = min(4, nj)
    steps = 3 * nj
    rest_end = lead - 1 + 2 * (nj - lead) + lead
    turns = max(steps + -(-LAG // SUB) + 9 * (half - 1), rest_end + n_tp + 5)

    def rows(j):
        return pl.ds(pl.multiple_of(j * CH, CH), CH)

    def piece(i):
        return pl.ds(pl.multiple_of(i * HALF, HALF), HALF)

    def unit(i):
        v, h = lax.div(i, SUB), lax.rem(i, SUB)
        a = v - lead
        b = a - 3 * (nj - lead)
        m = lax.rem(a, 3)
        mid = a < 3 * (nj - lead)
        first = a < 0
        k = jnp.where(first, 0, jnp.where(mid, jnp.where(m == 2, 0, m + 1), 1 + lax.rem(b, 2)))
        j = jnp.where(first, v, jnp.where(
            mid, lax.div(a, 3) + jnp.where(m == 2, lead, 0), nj - lead + lax.div(b, 2)))
        return SUB * j + h, k

    def fs_peer(d):
        return lax.rem(fs + d, n_fs)

    def tp_peer(d):
        return lax.rem(tp + d, n_tp)

    def load_gate(j):
        return pltpu.make_async_copy(gate_in.at[:, rows(j)], gate.at[:, rows(j)], gl_sem.at[j])

    def load_up(j):
        return pltpu.make_async_copy(up_in.at[:, rows(j)], up.at[:, rows(j)], ul_sem.at[j])

    def load_wd(j):
        return pltpu.make_async_copy(wd_in.at[rows(j), :], wd.at[fs, rows(j), :], wl_sem.at[j])

    def send_wd(j, d):
        return pltpu.make_async_remote_copy(
            src_ref=wd_in.at[rows(j), :], dst_ref=wd.at[fs, rows(j), :],
            send_sem=ws_sem.at[d - 1], recv_sem=wr_sem.at[d - 1, j],
            device_id={"fs": fs_peer(d)}, device_id_type=MESH)

    def recv_wd(j, d):
        src = lax.rem(fs + n_fs - d, n_fs)
        return pltpu.make_async_remote_copy(
            src_ref=wd_in.at[rows(j), :], dst_ref=wd.at[src, rows(j), :],
            send_sem=ws_sem.at[d - 1], recv_sem=wr_sem.at[d - 1, j],
            device_id={"fs": fs_peer(d)}, device_id_type=MESH)

    def x_copy(d, slot):
        return pltpu.make_async_remote_copy(
            src_ref=x_in, dst_ref=xb.at[slot], send_sem=xs_sem.at[d - 1], recv_sem=xr_sem.at[d - 1],
            device_id={"tp": tp_peer(d)}, device_id_type=MESH)

    def term_copy(d):
        return pltpu.make_async_remote_copy(
            src_ref=terms.at[tp_peer(d)], dst_ref=terms_in.at[d - 1],
            send_sem=ts_sem.at[d - 1], recv_sem=tr_sem.at[d - 1],
            device_id={"tp": tp_peer(d)}, device_id_type=MESH)

    def taps_copy(d, slot):
        return pltpu.make_async_remote_copy(
            src_ref=taps_all.at[rep], dst_ref=taps_all.at[slot],
            send_sem=ps_sem.at[d - 1], recv_sem=pr_sem.at[d - 1],
            device_id={"rep": lax.rem(rep + d, n_rep)}, device_id_type=MESH)

    def in_copy(j, k, dst):
        return pltpu.make_async_remote_copy(
            src_ref=part.at[k, piece(j), :], dst_ref=dst.at[k, piece(j), :],
            send_sem=in_s.at[k], recv_sem=(in_r if dst is from_out else out_r).at[k, j],
            device_id={"rep": inward}, device_id_type=MESH)

    def out_copy(j, k):
        return pltpu.make_async_remote_copy(
            src_ref=from_in.at[k, piece(j), :], dst_ref=from_in.at[k, piece(j), :],
            send_sem=out_s.at[k], recv_sem=out_r.at[k, j],
            device_id={"rep": outward}, device_id_type=MESH)

    def og_copy(d):
        cols = pl.ds(pl.multiple_of(fs_peer(d) * dw, dw), dw)
        return pltpu.make_async_copy(og_in.at[:, cols], og.at[:, cols], ld_sem.at[4 + d])

    loads = [
        pltpu.make_async_copy(taps_in, wt, ld_sem.at[0]),
        pltpu.make_async_copy(wg_in, wg, ld_sem.at[1]),
        pltpu.make_async_copy(wu_in, wu, ld_sem.at[2]),
        pltpu.make_async_copy(x_in, xb.at[tp], ld_sem.at[3]),
    ]
    taps_own[...] = jnp.zeros_like(taps_own)
    load_gate(0).start()
    load_up(0).start()
    loads[0].start()
    og_copy(0).start()

    barrier = pltpu.get_barrier_semaphore()
    for axis, n, me in (("rep", n_rep, rep), ("fs", n_fs, fs), ("tp", n_tp, tp)):
        for d in range(1, n):
            pl.semaphore_signal(barrier, inc=1, device_id={axis: lax.rem(me + d, n)}, device_id_type=MESH)
    for d in range(1, n_fs):
        og_copy(d).start()

    pos = lax.broadcasted_iota(jnp.int32, (seq, CH), 0)

    def back(v, n):
        return jnp.where(pos >= n, pltpu.roll(v, n, 0), 0.0)

    def ahead(v, n):
        return jnp.where(pos < seq - n, pltpu.roll(v, seq - n, 0), 0.0)

    def conv(j):
        g = gate[:, rows(j)].astype(F32)
        t = wt[:, rows(j)].astype(F32)
        b1, b2 = back(g, 1), back(g, 2)
        return g, b1, b2, t, t[0:1] * b2 + t[1:2] * b1 + t[2:3] * g

    tdot = functools.partial(lax.dot_general, dimension_numbers=(((0,), (0,)), ((), ())),
                             preferred_element_type=F32)
    wdot = functools.partial(lax.dot_general, dimension_numbers=(((1,), (1,)), ((), ())),
                             preferred_element_type=F32)

    own = pl.ds(pl.multiple_of(fs * dw, dw), dw)

    def down_first(j):
        load_gate(j).wait()
        load_up(j).wait()
        co = conv(j)[4]
        act[...] = (co * jax.nn.sigmoid(co) * up[:, rows(j)].astype(F32)).astype(BF16)

    def down_second(j):
        part[0, rows(j), :] = tdot(act[...], og[:, own]).astype(BF16)

    def rest_first(j):
        load_wd(j).wait()
        for d in range(1, n_fs):
            recv_wd(j, d).wait_recv()
        ag = wdot(og[:, 0:dw], wd[0, rows(j), :])
        for f in range(1, n_fs):
            ag = ag + wdot(og[:, f * dw:(f + 1) * dw], wd[f, rows(j), :])
        g, b1, b2, t, co = conv(j)
        s = jax.nn.sigmoid(co)
        upp[:, rows(j)] = (ag * (co * s)).astype(BF16)
        cg = ag * up[:, rows(j)].astype(F32) * s * (1.0 + co * (1.0 - s))
        gp[:, rows(j)] = (t[0:1] * ahead(cg, 2) + t[1:2] * ahead(cg, 1) + t[2:3] * cg).astype(BF16)
        for k, v in enumerate((b2, b1, g)):
            taps_own[pl.ds(3 * j + k, 1), :] = jnp.sum(cg * v, axis=0, keepdims=True)

    def rest_second(j):
        @pl.when(j == 0)
        def _():
            loads[3].wait()
            for d in range(1, n_tp):
                x_copy(d, lax.rem(tp + n_tp - d, n_tp)).wait_recv()
        g_part, u_part = gp[:, rows(j)], upp[:, rows(j)]
        for b in range(n_tp):
            part[1, rows(j), b * w:(b + 1) * w] = tdot(g_part, xb[b]).astype(BF16)
            part[2, rows(j), b * w:(b + 1) * w] = tdot(u_part, xb[b]).astype(BF16)

    def term_half(d, h):
        if h == 0:
            @pl.when(d == 1)
            def _():
                taps_all[rep] = taps_own[...].astype(BF16)
                for p in range(1, n_rep):
                    taps_copy(p, rep).start()
                loads[1].wait()
                loads[2].wait()
        b = tp_peer(d)
        r = pl.ds(pl.multiple_of(b * w, w), w)
        t = pl.ds(h * (seq // 2), seq // 2)
        terms[b, t, :] = (wdot(gp[t, :], wg[r, :]) + wdot(upp[t, :], wu[r, :])).astype(BF16)
        if h == 1:
            @pl.when(d < n_tp)
            def _():
                term_copy(d).start()

    def finish():
        total = terms[tp].astype(F32)
        for d in range(1, n_tp):
            term_copy(d).wait_recv()
            total = total + terms_in[d - 1].astype(F32)
        ig_out[...] = total.astype(BF16)
        for d in range(1, n_rep):
            taps_copy(d, lax.rem(rep + n_rep - d, n_rep)).wait_recv()
        acc = taps_all[0].astype(F32)
        for i in range(1, n_rep):
            acc = acc + taps_all[i].astype(F32)
        taps_own[...] = acc
        for j in range(nj):
            taps_out[0:3, j * CH:(j + 1) * CH] = taps_own[3 * j:3 * j + 3, :]
        for d in range(1, n_tp):
            x_copy(d, tp).wait_send()
            term_copy(d).wait_send()
        for d in range(1, n_rep):
            taps_copy(d, rep).wait_send()
        for d in range(1, n_fs):
            pltpu.make_async_remote_copy(
                src_ref=wd_in, dst_ref=wd.at[fs], send_sem=ws_sem.at[d - 1], recv_sem=wr_sem.at[d - 1, 0],
                device_id={"fs": fs_peer(d)}, device_id_type=MESH).wait_send()

    def q_stage(j, k):
        @pl.when(has_out)
        def _():
            in_copy(j, k, from_out).wait_recv()
            r = piece(j)
            part[k, r, :] = (part[k, r, :].astype(F32) + from_out[k, r, :].astype(F32)).astype(BF16)

        @pl.when(innermost)
        def _():
            in_copy(j, k, from_in).start()

        @pl.when(jnp.logical_not(innermost))
        def _():
            in_copy(j, k, from_out).start()

    def s_stage(j, k):
        out_copy(j, k).wait_recv()

        @pl.when(innermost)
        def _():
            r = piece(j)
            from_in[k, r, :] = (part[k, r, :].astype(F32) + from_in[k, r, :].astype(F32)).astype(BF16)

        @pl.when(has_out)
        def _():
            out_copy(j, k).start()

    def load_rest(j, c):
        load_gate(j).start()
        load_up(j).start()
        return c
    lax.fori_loop(1, nj, load_rest, 0)
    loads[0].wait()
    down_first(0)
    og_copy(0).wait()
    down_second(0)
    pl.semaphore_wait(barrier, n_rep + n_fs + n_tp - 3)

    @pl.when(jnp.logical_not(has_out))
    def _():
        for h in range(SUB):
            q_stage(h, 0)
    for d in range(1, n_tp):
        x_copy(d, tp).start()

    def weights(j, c):
        for d in range(1, n_fs):
            send_wd(j, d).start()
        load_wd(j).start()
        return c
    lax.fori_loop(0, nj, weights, 0)
    for load in loads[1:]:
        load.start()
    for d in range(1, n_fs):
        og_copy(d).wait()

    def step(v, c):
        a = v - (lead - 1)
        b = a - 2 * (nj - lead)
        early = a < 0
        mid = jnp.logical_and(a >= 0, b < 0)
        is_down = jnp.logical_or(early, jnp.logical_and(mid, lax.rem(a, 2) == 1))
        is_rest = jnp.logical_and(jnp.logical_not(is_down), b < lead)
        is_term = jnp.logical_and(b >= lead, b < lead + n_tp)
        down_j = jnp.where(early, v + 1, lead + lax.div(a, 2))
        rest_j = jnp.where(mid, lax.div(a, 2), nj - lead + b)
        for h in range(SUB):
            i = SUB * v + h

            @pl.when(jnp.logical_and(v < steps, jnp.logical_or(v > 0, has_out)))
            def _():
                q_stage(*unit(i))
            si = i - lag

            @pl.when(jnp.logical_and(si >= 0, si < SUB * steps))
            def _():
                s_stage(*unit(si))

            turn = {0: 0, SUB // 2: 1}.get(h)
            if turn is None:
                continue

            @pl.when(is_down)
            def _():
                (down_first, down_second)[turn](down_j)

            @pl.when(is_rest)
            def _():
                (rest_first, rest_second)[turn](rest_j)

            @pl.when(is_term)
            def _():
                term_half(b - lead + 1, turn)

        @pl.when(v == rest_end + n_tp + 4)
        def _():
            finish()
        return c
    lax.fori_loop(0, turns, step, 0)

    for k in range(3):
        pltpu.make_async_remote_copy(
            src_ref=part.at[k], dst_ref=from_out.at[k], send_sem=in_s.at[k], recv_sem=in_r.at[k, 0],
            device_id={"rep": inward}, device_id_type=MESH).wait_send()

        @pl.when(has_out)
        def _():
            pltpu.make_async_remote_copy(
                src_ref=from_in.at[k], dst_ref=from_in.at[k], send_sem=out_s.at[k], recv_sem=out_r.at[k, 0],
                device_id={"rep": outward}, device_id_type=MESH).wait_send()


def widen(grads, input_grad, taps, ig_out, gate_out, up_out, down_out, taps_out, ring, ring_t, d_sem, t_sem, s_sem):
    hid, dw = down_out.shape
    slots = ring.shape[0]
    small = [
        pltpu.make_async_copy(input_grad, ig_out, s_sem.at[0]),
        pltpu.make_async_copy(taps.at[0:3, :], taps_out, s_sem.at[1]),
    ]
    for copy in small:
        copy.start()

    def down(i, s):
        return pltpu.make_async_copy(ring.at[s], down_out.at[pl.ds(i * WIDE, WIDE), :], d_sem.at[s])

    def wide(out, i, s):
        return pltpu.make_async_copy(ring_t.at[s], out.at[:, pl.ds(i * WIDE, WIDE)], t_sem.at[s])

    n = hid // WIDE
    for i in range(n):
        r = slice(i * WIDE, (i + 1) * WIDE)
        s = i % slots
        if i >= slots:
            down(i - slots, s).wait()
            wide(gate_out, i - slots, 2 * s).wait()
            wide(up_out, i - slots, 2 * s + 1).wait()
        ring[s] = grads[0, r, :].astype(F32)
        down(i, s).start()
        ring_t[2 * s] = grads[1, r, :].astype(F32).T
        wide(gate_out, i, 2 * s).start()
        ring_t[2 * s + 1] = grads[2, r, :].astype(F32).T
        wide(up_out, i, 2 * s + 1).start()
    for i in range(max(n - slots, 0), n):
        s = i % slots
        down(i, s).wait()
        wide(gate_out, i, 2 * s).wait()
        wide(up_out, i, 2 * s + 1).wait()
    for copy in small:
        copy.wait()


def solution(mesh):
    n_rep, n_fs, n_tp = mesh.shape["rep"], mesh.shape["fs"], mesh.shape["tp"]

    def local(layer_input, gate_saved, up_saved, out_grad, conv_taps, w_gate, w_up, w_down):
        seq, w = layer_input.shape
        dw, hid = w_gate.shape
        width = out_grad.shape[1]
        nj = hid // CH
        tap_rows = -(-3 * nj // 16) * 16
        any_spec = pl.BlockSpec(memory_space=pl.ANY)
        vmem = pl.BlockSpec(memory_space=pltpu.VMEM)
        dma = pltpu.SemaphoreType.DMA
        grads, input_grad, taps = pl.pallas_call(
            functools.partial(kernel, n_rep, n_fs, n_tp),
            out_shape=(
                pltpu.VMEM((3, hid, dw), BF16),
                pltpu.VMEM((seq, w), BF16),
                pltpu.VMEM((8, hid), F32),
            ),
            in_specs=[any_spec] * 8,
            out_specs=(vmem, vmem, vmem),
            scratch_shapes=[
                pltpu.VMEM((n_tp, seq, w), BF16),
                pltpu.VMEM((seq, hid), BF16),
                pltpu.VMEM((seq, hid), BF16),
                pltpu.VMEM((seq, width), BF16),
                pltpu.VMEM((3, hid), BF16),
                pltpu.VMEM((dw, hid), BF16),
                pltpu.VMEM((dw, hid), BF16),
                pltpu.VMEM((n_fs, hid, dw), BF16),
                pltpu.VMEM((seq, CH), BF16),
                pltpu.VMEM((3, hid, dw), BF16),
                pltpu.VMEM((3, hid, dw), BF16),
                pltpu.VMEM((seq, hid), BF16),
                pltpu.VMEM((seq, hid), BF16),
                pltpu.VMEM((n_tp, seq, w), BF16),
                pltpu.VMEM((n_tp - 1, seq, w), BF16),
                pltpu.VMEM((tap_rows, CH), F32),
                pltpu.VMEM((n_rep, tap_rows, CH), BF16),
                dma((n_tp - 1,)),
                dma((n_tp - 1,)),
                dma((nj,)),
                dma((nj,)),
                dma((4 + n_fs,)),
                dma((nj,)),
                dma((n_fs - 1,)),
                dma((n_fs - 1, nj)),
                dma((3,)),
                dma((3, SUB * nj)),
                dma((3,)),
                dma((3, SUB * nj)),
                dma((n_tp - 1,)),
                dma((n_tp - 1,)),
                dma((n_rep - 1,)),
                dma((n_rep - 1,)),
            ],
            compiler_params=pltpu.CompilerParams(
                collective_id=0, has_side_effects=True, vmem_limit_bytes=52 * 2**20
            ),
        )(layer_input, gate_saved, up_saved, out_grad, conv_taps, w_gate, w_up, w_down)
        grads, input_grad, taps = (pltpu.with_memory_space_constraint(v, pltpu.VMEM) for v in (grads, input_grad, taps))
        slots = min(4, hid // WIDE)
        return pl.pallas_call(
            widen,
            out_shape=(
                jax.ShapeDtypeStruct((seq, w), BF16),
                jax.ShapeDtypeStruct((dw, hid), F32),
                jax.ShapeDtypeStruct((dw, hid), F32),
                jax.ShapeDtypeStruct((hid, dw), F32),
                jax.ShapeDtypeStruct((3, hid), F32),
            ),
            in_specs=[vmem] * 3,
            out_specs=[any_spec] * 5,
            scratch_shapes=[
                pltpu.VMEM((slots, WIDE, dw), F32),
                pltpu.VMEM((2 * slots, dw, WIDE), F32),
                dma((slots,)),
                dma((2 * slots,)),
                dma((2,)),
            ],
            compiler_params=pltpu.CompilerParams(vmem_limit_bytes=24 * 2**20),
        )(grads, input_grad, taps)

    return jax.shard_map(
        local,
        mesh=mesh,
        in_specs=(
            P("rep", ("fs", "tp")), P("rep", "tp"), P("rep", "tp"), P("rep", None),
            P(None, "tp"), P("fs", "tp"), P("fs", "tp"), P("tp", "fs"),
        ),
        out_specs=(P("rep", ("fs", "tp")), P("fs", "tp"), P("fs", "tp"), P("tp", "fs"), P(None, "tp")),
        check_vma=False,
    )
```

time: 201 us -> 193 us (0.960)
  Pallas kernels: 200 us -> 192 us
    pallas_call x1, Pallas kernels: 193 us -> 186 us  [local(): pl.pallas_call(functools.partial(kernel, n_rep, n_fs, n_tp), out_shape=(p...]
where the time goes in v2:
time: 193 us
  Pallas kernels  192 us (99%)
    pallas_call x1, Pallas kernels, local(): pl.pallas_call(functools.partial(kernel, n_rep, n_fs, n_tp), out_shape=(p...  186 us
    pallas_call x1, Pallas kernels, local(): pl.pallas_call(widen, out_shape=(jax.ShapeDtypeStruct((seq, w), BF16), ja...  5.88 us

profile of v2, /device:TPU:0, one launch (start us, length us, event | category | flops | bytes accessed | tf_op | source)
XLA Modules:
  0.0 192.9 jit_solution(5212791832420503028)
XLA Ops:
  0.6 186.3 %shard_map.119 = (bf16[3,1280,1024]{2,1,0:T(8,128)(2,1)S(1)}, bf16[768,256]{1,0:T(8,128)(2,1)S(1)}, f32[8,1280]{1,0:T(8,128)S(1)}) custom-call(bf16[768,256]{1,0:T(8,128)(2,1)} %x_in.1, bf16[768,1280]{1,0:T(8,128)(2,1)} %gate_in.1, bf16[768,1280]{1,0:T(8,128)(2,1)} %up_in.1, bf16[768,2048]{1,0:T(8,128)(2,1)} %og_in.1, bf16[3,1280]{1,0:T(4,128)(2,1)} %taps_in.1, ...), custom_call_target="tpu_custom_call" | custom-call | tf_op jit(solution)/shard_map/pallas_call | solution.py:403
  187.0 5.9 %shard_map.120 = (bf16[768,256]{1,0:T(8,128)(2,1)}, f32[1024,1280]{1,0:T(8,128)}, f32[1024,1280]{1,0:T(8,128)}, f32[1280,1024]{1,0:T(8,128)}, f32[3,1280]{1,0:T(4,128)}) custom-call(bf16[3,1280,1024]{2,1,0:T(8,128)(2,1)S(1)} %get-tuple-element.8.grads, bf16[768,256]{1,0:T(8,128)(2,1)S(1)} %get-tuple-element.9.input_grad, f32[8,1280]{1,0:T(8,128)S(1)} %get-tuple-element.10.taps), custom_call_target="tpu_custom_call" | custom-call | tf_op jit(solution)/shard_map/pallas_call | solution.py:453

commit v3 on v2

--- a/solution.py
+++ b/solution.py
@@ -13,7 +13,8 @@
 CH = 128
 SUB = 4
 HALF = CH // SUB
-LAG = 3
+LAG = 2
+HOP = 3
 WIDE = 128
 
 
@@ -35,11 +36,12 @@
     has_out = depth > 0
     outward = jnp.where(has_out, outward, inward)
     innermost = depth == half - 1
-    lag = LAG + 9 * SUB * (half - 1 - depth)
+    lag = LAG + HOP * SUB * (half - 1 - depth)
     lead = min(4, nj)
     steps = 3 * nj
+    ring = in_r.shape[0]
     rest_end = lead - 1 + 2 * (nj - lead) + lead
-    turns = max(steps + -(-LAG // SUB) + 9 * (half - 1), rest_end + n_tp + 5)
+    turns = max(steps + -(-LAG // SUB) + HOP * (half - 1), rest_end + n_tp + 5)
 
     def rows(j):
         return pl.ds(pl.multiple_of(j * CH, CH), CH)
@@ -65,14 +67,15 @@
     def tp_peer(d):
         return lax.rem(tp + d, n_tp)
 
-    def load_gate(j):
-        return pltpu.make_async_copy(gate_in.at[:, rows(j)], gate.at[:, rows(j)], gl_sem.at[j])
-
-    def load_up(j):
-        return pltpu.make_async_copy(up_in.at[:, rows(j)], up.at[:, rows(j)], ul_sem.at[j])
-
-    def load_wd(j):
-        return pltpu.make_async_copy(wd_in.at[rows(j), :], wd.at[fs, rows(j), :], wl_sem.at[j])
+    def load_gate(p):
+        c = slice(0, CH) if p == 0 else slice(CH, hid)
+        return pltpu.make_async_copy(gate_in.at[:, c], gate.at[:, c], gl_sem.at[p])
+
+    def load_up(p):
+        c = slice(0, CH) if p == 0 else slice(CH, hid)
+        return pltpu.make_async_copy(up_in.at[:, c], up.at[:, c], ul_sem.at[p])
+
+    load_wd = pltpu.make_async_copy(wd_in, wd.at[fs], wl_sem.at[0])
 
     def send_wd(j, d):
         return pltpu.make_async_remote_copy(
@@ -104,16 +107,16 @@
             send_sem=ps_sem.at[d - 1], recv_sem=pr_sem.at[d - 1],
             device_id={"rep": lax.rem(rep + d, n_rep)}, device_id_type=MESH)
 
-    def in_copy(j, k, dst):
+    def in_copy(i, j, k, dst):
         return pltpu.make_async_remote_copy(
             src_ref=part.at[k, piece(j), :], dst_ref=dst.at[k, piece(j), :],
-            send_sem=in_s.at[k], recv_sem=(in_r if dst is from_out else out_r).at[k, j],
+            send_sem=in_s.at[k], recv_sem=(in_r if dst is from_out else out_r).at[lax.rem(i, ring)],
             device_id={"rep": inward}, device_id_type=MESH)
 
-    def out_copy(j, k):
+    def out_copy(i, j, k):
         return pltpu.make_async_remote_copy(
             src_ref=from_in.at[k, piece(j), :], dst_ref=from_in.at[k, piece(j), :],
-            send_sem=out_s.at[k], recv_sem=out_r.at[k, j],
+            send_sem=out_s.at[k], recv_sem=out_r.at[lax.rem(i, ring)],
             device_id={"rep": outward}, device_id_type=MESH)
 
     def og_copy(d):
@@ -161,8 +164,10 @@
     own = pl.ds(pl.multiple_of(fs * dw, dw), dw)
 
     def down_first(j):
-        load_gate(j).wait()
-        load_up(j).wait()
+        @pl.when(j == 1)
+        def _():
+            load_gate(1).wait()
+            load_up(1).wait()
         co = conv(j)[4]
         act[...] = (co * jax.nn.sigmoid(co) * up[:, rows(j)].astype(F32)).astype(BF16)
 
@@ -170,7 +175,9 @@
         part[0, rows(j), :] = tdot(act[...], og[:, own]).astype(BF16)
 
     def rest_first(j):
-        load_wd(j).wait()
+        @pl.when(j == 0)
+        def _():
+            load_wd.wait()
         for d in range(1, n_fs):
             recv_wd(j, d).wait_recv()
         ag = wdot(og[:, 0:dw], wd[0, rows(j), :])
@@ -237,23 +244,26 @@
                 src_ref=wd_in, dst_ref=wd.at[fs], send_sem=ws_sem.at[d - 1], recv_sem=wr_sem.at[d - 1, 0],
                 device_id={"fs": fs_peer(d)}, device_id_type=MESH).wait_send()
 
-    def q_stage(j, k):
+    def q_stage(i):
+        j, k = unit(i)
+
         @pl.when(has_out)
         def _():
-            in_copy(j, k, from_out).wait_recv()
+            in_copy(i, j, k, from_out).wait_recv()
             r = piece(j)
             part[k, r, :] = (part[k, r, :].astype(F32) + from_out[k, r, :].astype(F32)).astype(BF16)
 
         @pl.when(innermost)
         def _():
-            in_copy(j, k, from_in).start()
+            in_copy(i, j, k, from_in).start()
 
         @pl.when(jnp.logical_not(innermost))
         def _():
-            in_copy(j, k, from_out).start()
-
-    def s_stage(j, k):
-        out_copy(j, k).wait_recv()
+            in_copy(i, j, k, from_out).start()
+
+    def s_stage(i):
+        j, k = unit(i)
+        out_copy(i, j, k).wait_recv()
 
         @pl.when(innermost)
         def _():
@@ -262,14 +272,13 @@
 
         @pl.when(has_out)
         def _():
-            out_copy(j, k).start()
-
-    def load_rest(j, c):
-        load_gate(j).start()
-        load_up(j).start()
-        return c
-    lax.fori_loop(1, nj, load_rest, 0)
+            out_copy(i, j, k).start()
+
+    load_gate(1).start()
+    load_up(1).start()
     loads[0].wait()
+    load_gate(0).wait()
+    load_up(0).wait()
     down_first(0)
     og_copy(0).wait()
     down_second(0)
@@ -278,15 +287,15 @@
     @pl.when(jnp.logical_not(has_out))
     def _():
         for h in range(SUB):
-            q_stage(h, 0)
+            q_stage(jnp.int32(h))
     for d in range(1, n_tp):
         x_copy(d, tp).start()
 
     def weights(j, c):
         for d in range(1, n_fs):
             send_wd(j, d).start()
-        load_wd(j).start()
         return c
+    load_wd.start()
     lax.fori_loop(0, nj, weights, 0)
     for load in loads[1:]:
         load.start()
@@ -308,28 +317,26 @@
 
             @pl.when(jnp.logical_and(v < steps, jnp.logical_or(v > 0, has_out)))
             def _():
-                q_stage(*unit(i))
+                q_stage(i)
+            turn = {0: 0, SUB // 2: 1}.get(h)
+            if turn is not None:
+                @pl.when(is_down)
+                def _():
+                    (down_first, down_second)[turn](down_j)
+
+                @pl.when(is_rest)
+                def _():
+                    (rest_first, rest_second)[turn](rest_j)
+
+                @pl.when(is_term)
+                def _():
+                    term_half(b - lead + 1, turn)
+
             si = i - lag
 
             @pl.when(jnp.logical_and(si >= 0, si < SUB * steps))
             def _():
-                s_stage(*unit(si))
-
-            turn = {0: 0, SUB // 2: 1}.get(h)
-            if turn is None:
-                continue
-
-            @pl.when(is_down)
-            def _():
-                (down_first, down_second)[turn](down_j)
-
-            @pl.when(is_rest)
-            def _():
-                (rest_first, rest_second)[turn](rest_j)
-
-            @pl.when(is_term)
-            def _():
-                term_half(b - lead + 1, turn)
+                s_stage(si)
 
         @pl.when(v == rest_end + n_tp + 4)
         def _():
@@ -339,13 +346,13 @@
 
     for k in range(3):
         pltpu.make_async_remote_copy(
-            src_ref=part.at[k], dst_ref=from_out.at[k], send_sem=in_s.at[k], recv_sem=in_r.at[k, 0],
+            src_ref=part.at[k], dst_ref=from_out.at[k], send_sem=in_s.at[k], recv_sem=in_r.at[0],
             device_id={"rep": inward}, device_id_type=MESH).wait_send()
 
         @pl.when(has_out)
         def _():
             pltpu.make_async_remote_copy(
-                src_ref=from_in.at[k], dst_ref=from_in.at[k], send_sem=out_s.at[k], recv_sem=out_r.at[k, 0],
+                src_ref=from_in.at[k], dst_ref=from_in.at[k], send_sem=out_s.at[k], recv_sem=out_r.at[0],
                 device_id={"rep": outward}, device_id_type=MESH).wait_send()
 
 
@@ -396,6 +403,7 @@
         dw, hid = w_gate.shape
         width = out_grad.shape[1]
         nj = hid // CH
+        ring = min(LAG + HOP * SUB * (n_rep // 2 - 1) + 2, 3 * SUB * nj)
         tap_rows = -(-3 * nj // 16) * 16
         any_spec = pl.BlockSpec(memory_space=pl.ANY)
         vmem = pl.BlockSpec(memory_space=pltpu.VMEM)
@@ -429,16 +437,16 @@
                 pltpu.VMEM((n_rep, tap_rows, CH), BF16),
                 dma((n_tp - 1,)),
                 dma((n_tp - 1,)),
-                dma((nj,)),
-                dma((nj,)),
+                dma((2,)),
+                dma((2,)),
                 dma((4 + n_fs,)),
-                dma((nj,)),
+                dma((1,)),
                 dma((n_fs - 1,)),
                 dma((n_fs - 1, nj)),
                 dma((3,)),
-                dma((3, SUB * nj)),
+                dma((ring,)),
                 dma((3,)),
-                dma((3, SUB * nj)),
+                dma((ring,)),
                 dma((n_tp - 1,)),
                 dma((n_tp - 1,)),
                 dma((n_rep - 1,)),

time: 193 us -> 191 us (0.990)
  Pallas kernels: 192 us -> 190 us
    pallas_call x1, Pallas kernels: 186 us -> 184 us  [local(): pl.pallas_call(functools.partial(kernel, n_rep, n_fs, n_tp), out_shape=(p...]
where the time goes in v3:
time: 191 us; the launch traced here: 190 us
  Pallas kernels  190 us (99%)
    pallas_call x1, Pallas kernels, local(): pl.pallas_call(functools.partial(kernel, n_rep, n_fs, n_tp), out_shape=(p...  184 us
    pallas_call x1, Pallas kernels, local(): pl.pallas_call(widen, out_shape=(jax.ShapeDtypeStruct((seq, w), BF16), ja...  5.88 us

profile of v3, /device:TPU:0, one launch (start us, length us, event | category | flops | bytes accessed | tf_op | source)
XLA Modules:
  0.0 190.4 jit_solution(5078331595642181982)
XLA Ops:
  0.6 183.9 %shard_map.119 = (bf16[3,1280,1024]{2,1,0:T(8,128)(2,1)S(1)}, bf16[768,256]{1,0:T(8,128)(2,1)S(1)}, f32[8,1280]{1,0:T(8,128)S(1)}) custom-call(bf16[768,256]{1,0:T(8,128)(2,1)} %x_in.1, bf16[768,1280]{1,0:T(8,128)(2,1)} %gate_in.1, bf16[768,1280]{1,0:T(8,128)(2,1)} %up_in.1, bf16[768,2048]{1,0:T(8,128)(2,1)} %og_in.1, bf16[3,1280]{1,0:T(4,128)(2,1)} %taps_in.1, ...), custom_call_target="tpu_custom_call" | custom-call | tf_op jit(solution)/shard_map/pallas_call | solution.py:411
  184.5 5.9 %shard_map.120 = (bf16[768,256]{1,0:T(8,128)(2,1)}, f32[1024,1280]{1,0:T(8,128)}, f32[1024,1280]{1,0:T(8,128)}, f32[1280,1024]{1,0:T(8,128)}, f32[3,1280]{1,0:T(4,128)}) custom-call(bf16[3,1280,1024]{2,1,0:T(8,128)(2,1)S(1)} %get-tuple-element.8.grads, bf16[768,256]{1,0:T(8,128)(2,1)S(1)} %get-tuple-element.9.input_grad, f32[8,1280]{1,0:T(8,128)S(1)} %get-tuple-element.10.taps), custom_call_target="tpu_custom_call" | custom-call | tf_op jit(solution)/shard_map/pallas_call | solution.py:461

commit v4 on v3

--- a/solution.py
+++ b/solution.py
@@ -251,7 +251,7 @@
         def _():
             in_copy(i, j, k, from_out).wait_recv()
             r = piece(j)
-            part[k, r, :] = (part[k, r, :].astype(F32) + from_out[k, r, :].astype(F32)).astype(BF16)
+            part[k, r, :] = part[k, r, :] + from_out[k, r, :]
 
         @pl.when(innermost)
         def _():
@@ -268,7 +268,7 @@
         @pl.when(innermost)
         def _():
             r = piece(j)
-            from_in[k, r, :] = (part[k, r, :].astype(F32) + from_in[k, r, :].astype(F32)).astype(BF16)
+            from_in[k, r, :] = part[k, r, :] + from_in[k, r, :]
 
         @pl.when(has_out)
         def _():

time: 191 us -> 191 us (level)
  no operation moved by 1% of the time
where the time goes in v4:
time: 191 us; the launch traced here: 190 us
  Pallas kernels  190 us (99%)
    pallas_call x1, Pallas kernels, local(): pl.pallas_call(functools.partial(kernel, n_rep, n_fs, n_tp), out_shape=(p...  184 us
    pallas_call x1, Pallas kernels, local(): pl.pallas_call(widen, out_shape=(jax.ShapeDtypeStruct((seq, w), BF16), ja...  5.88 us

profile of v4, /device:TPU:0, one launch (start us, length us, event | category | flops | bytes accessed | tf_op | source)
XLA Modules:
  0.0 190.4 jit_solution(12180570499151611824)
XLA Ops:
  0.6 183.9 %shard_map.119 = (bf16[3,1280,1024]{2,1,0:T(8,128)(2,1)S(1)}, bf16[768,256]{1,0:T(8,128)(2,1)S(1)}, f32[8,1280]{1,0:T(8,128)S(1)}) custom-call(bf16[768,256]{1,0:T(8,128)(2,1)} %x_in.1, bf16[768,1280]{1,0:T(8,128)(2,1)} %gate_in.1, bf16[768,1280]{1,0:T(8,128)(2,1)} %up_in.1, bf16[768,2048]{1,0:T(8,128)(2,1)} %og_in.1, bf16[3,1280]{1,0:T(4,128)(2,1)} %taps_in.1, ...), custom_call_target="tpu_custom_call" | custom-call | tf_op jit(solution)/shard_map/pallas_call | solution.py:411
  184.5 5.9 %shard_map.120 = (bf16[768,256]{1,0:T(8,128)(2,1)}, f32[1024,1280]{1,0:T(8,128)}, f32[1024,1280]{1,0:T(8,128)}, f32[1280,1024]{1,0:T(8,128)}, f32[3,1280]{1,0:T(4,128)}) custom-call(bf16[3,1280,1024]{2,1,0:T(8,128)(2,1)S(1)} %get-tuple-element.8.grads, bf16[768,256]{1,0:T(8,128)(2,1)S(1)} %get-tuple-element.9.input_grad, f32[8,1280]{1,0:T(8,128)S(1)} %get-tuple-element.10.taps), custom_call_target="tpu_custom_call" | custom-call | tf_op jit(solution)/shard_map/pallas_call | solution.py:461
